TPU v7x, 32 devices: a whole 2x2x4 slice. The times are simulated.
32 devices in a mesh: grp: 2 (over y), sp: 4 (over z), tp: 4 (over x, core).
Axes of the slice: x: 2, y: 2, z: 4, core: 2. Of those that a mesh axis runs over, the one named last changes fastest.
Arguments:
- queries: bfloat16 [6144, 512], P(('grp', 'sp'), 'tp'), parts along dimension 0, may hold values from -6 to 6
- key_projected: bfloat16 [6144, 512], P(('grp', 'sp'), 'tp'), parts along dimension 0, may hold values from -6 to 6
- values: bfloat16 [6144, 1024], P(('grp', 'sp'), 'tp'), parts along dimension 0, may hold values from -6 to 6
- output_gate_preact: bfloat16 [6144, 1024], P(('grp', 'sp'), 'tp'), parts along dimension 0, may hold values from -6 to 6
- forward_decay_logits: bfloat16 [6144, 512], P(('grp', 'sp'), 'tp'), parts along dimension 0, may hold values from -3.8 to 3.8
- backward_decay_logits: bfloat16 [6144, 512], P(('grp', 'sp'), 'tp'), parts along dimension 0, may hold values from -3.8 to 3.8
- decay_logit_shift: float32 [2, 512], P(None, 'tp'), may hold values from -1 to 13
- decay_spike_values: float32 [8, 6144], P('tp', ('grp', 'sp')), parts along dimension 1, may hold values from -2.1 to 0
- residual: bfloat16 [6144, 2048], P(('grp', 'sp', 'tp')), parts along dimension 0, may hold values from -6 to 6
- head_norm_gain: float32 [1024], P('tp'), may hold values from 0.1 to 1.9
- output_projection: bfloat16 [1024, 2048], P('tp'), may hold values from -0.1875 to 0.1875
- prenorm_gain: float32 [2048], replicated, may hold values from 0.1 to 1.9
- gate_projection: bfloat16 [2048, 5120], P('sp', 'tp'), may hold values from -0.125 to 0.125
- up_projection: bfloat16 [2048, 5120], P('sp', 'tp'), may hold values from -0.125 to 0.125
- down_projection: bfloat16 [5120, 2048], P('tp', 'sp'), may hold values from -0.078125 to 0.078125
Outputs:
- layer_output: bfloat16 [6144, 2048], P(('grp', 'sp', 'tp')), parts along dimension 0
There are 2 independent parts, one for each index of `grp`. A program takes and returns all parts, laid end to end along the dimension named above; an argument that names none is the same for every part. Nothing has to cross between parts.
All inputs are finite; a program needn't handle non-finite values.
Results may differ from a plain program's by a relative error of at most 0.014.
Values may be sent and summed in bfloat16 or wider, within the bound.
A program may use at most 64 MiB of HBM per device.

v0:
```python
import jax
import jax.numpy as jnp
from jax import lax
from jax.sharding import PartitionSpec as P

KEY_CHANNELS = 64
HEAD_V = 128
BLOCK = 64
gate_denominator = 16.0
norm_epsilon = 1e-06


def entering(value, axis, join, neutral, backward):
    count = lax.axis_size(axis)
    place = lax.axis_index(axis)
    ahead = count - 1 - place if backward else place
    gathered = jax.tree.map(
        lambda a, kind: lax.all_gather(a.astype(kind), axis), value, (jnp.bfloat16, jnp.bfloat16)
    )
    state = jax.tree.map(lambda a, e: jnp.zeros_like(a) + jnp.asarray(e, a.dtype), value, neutral)

    def one(lap, state):
        source = count - 1 - lap if backward else lap
        return join(
            state,
            jax.tree.map(
                lambda a, own: lax.dynamic_index_in_dim(a, source, 0, False).astype(own.dtype),
                gathered,
                value,
            ),
        )

    return lax.fori_loop(0, ahead, one, state)


def block_sweep(query_in, key_in, values_in, log_decay, span):
    sequence_length, head_count, key_dim = key_in.shape
    block_count = sequence_length // span

    def blocks(tensor):
        return jnp.transpose(
            tensor.reshape(block_count, span, head_count, tensor.shape[-1]), (0, 2, 1, 3)
        )

    lower_mask = jnp.tril(jnp.ones((span, span), dtype=bool))[:, :, None]

    def advance(carried, inputs):
        memory, offset = carried
        key_blk, value_blk, decay_blk, query_blk = inputs
        within = jnp.cumsum(decay_blk, axis=1)
        ending = within[:, -1, :]
        memory_next = jnp.exp(ending)[:, :, None] * memory + jnp.einsum(
            "hjd,hje->hde",
            key_blk * jnp.exp(ending[:, None, :] - within),
            value_blk,
            precision=lax.Precision.HIGHEST,
        )
        result = jnp.einsum(
            "hid,hde->hie", query_blk * jnp.exp(within), memory, precision=lax.Precision.HIGHEST
        )
        spread = jnp.exp(
            jnp.where(lower_mask, within[:, :, None, :] - within[:, None, :, :], -jnp.inf)
        )
        scores = jnp.einsum(
            "hid,hjd,hijd->hij", query_blk, key_blk, spread, precision=lax.Precision.HIGHEST
        )
        result = result + jnp.einsum(
            "hij,hje->hie", scores, value_blk, precision=lax.Precision.HIGHEST
        )
        reached = query_blk * jnp.exp(within + offset[:, None, :])
        return ((memory_next, offset + ending), (result, reached))

    start_memory = jnp.zeros((head_count, key_dim, values_in.shape[-1]), jnp.float32)
    start_offset = jnp.zeros((head_count, key_dim), jnp.float32)
    (memory, decay_total), (outputs, reached) = lax.scan(
        advance,
        (start_memory, start_offset),
        (blocks(key_in), blocks(values_in), blocks(log_decay), blocks(query_in)),
    )

    def unblock(tensor):
        return jnp.transpose(tensor, (0, 2, 1, 3)).reshape(
            sequence_length, head_count, tensor.shape[-1]
        )

    return (unblock(outputs), unblock(reached), memory, decay_total)


def head_mix(combined, head_norm_gain, output_gate_preact):
    sequence_length, head_count, width = combined.shape
    inverse = lax.rsqrt(jnp.mean(combined * combined, axis=-1, keepdims=True) + norm_epsilon)
    gate_act = jax.nn.silu(
        output_gate_preact.astype(jnp.float32).reshape(sequence_length, head_count, width)
    )
    weighted = combined * inverse * head_norm_gain.reshape(head_count, width) * gate_act
    return weighted.reshape(sequence_length, head_count * width).astype(jnp.bfloat16)


def row_norm(mid_rows, prenorm_gain):
    wide = mid_rows.astype(jnp.float32)
    inverse = lax.rsqrt(jnp.mean(wide * wide, axis=-1, keepdims=True) + norm_epsilon)
    return (wide * inverse * prenorm_gain).astype(jnp.bfloat16)


def combine_states(earlier, later):
    decay_early, memory_early = earlier
    decay_late, memory_late = later
    return (decay_early * decay_late, decay_late[:, :, None] * memory_early + memory_late)


def body(
    queries,
    key_projected,
    values,
    output_gate_preact,
    forward_decay_logits,
    backward_decay_logits,
    decay_logit_shift,
    decay_spike_values,
    residual,
    head_norm_gain,
    output_projection,
    prenorm_gain,
    gate_projection,
    up_projection,
    down_projection,
):
    sequence_length = queries.shape[0]
    local_heads = queries.shape[1] // KEY_CHANNELS
    query_f = queries.astype(jnp.float32).reshape(
        sequence_length, local_heads, KEY_CHANNELS
    ) * KEY_CHANNELS ** (-0.5)
    keys_f = key_projected.astype(jnp.float32).reshape(sequence_length, local_heads, KEY_CHANNELS)
    values_f = values.astype(jnp.float32).reshape(sequence_length, local_heads, HEAD_V)
    decay_spikes = jnp.transpose(decay_spike_values)[:, :, None]
    logit_shifts = decay_logit_shift.reshape(2, local_heads, KEY_CHANNELS)
    forward_decay = (
        jax.nn.log_sigmoid(
            forward_decay_logits.astype(jnp.float32).reshape(
                sequence_length, local_heads, KEY_CHANNELS
            )
            + logit_shifts[0]
        )
        / gate_denominator
        + decay_spikes
    )
    backward_decay = (
        jax.nn.log_sigmoid(
            backward_decay_logits.astype(jnp.float32).reshape(
                sequence_length, local_heads, KEY_CHANNELS
            )
            + logit_shifts[1]
        )
        / gate_denominator
        + decay_spikes
    )
    fwd_out, fwd_reach, fwd_memory, fwd_total = block_sweep(
        query_f, keys_f, values_f, forward_decay, BLOCK
    )
    bwd_out, bwd_reach, bwd_memory, bwd_total = block_sweep(
        query_f[::-1], keys_f[::-1], values_f[::-1], backward_decay[::-1], BLOCK
    )
    identity = (jnp.ones_like(fwd_total), jnp.zeros_like(fwd_memory))
    fwd_incoming = entering(
        (jnp.exp(fwd_total), fwd_memory), "sp", combine_states, identity, False
    )[1]
    bwd_incoming = entering((jnp.exp(bwd_total), bwd_memory), "sp", combine_states, identity, True)[
        1
    ]
    fwd_full = fwd_out + jnp.einsum(
        "lhd,hde->lhe", fwd_reach, fwd_incoming, precision=lax.Precision.HIGHEST
    )
    bwd_full = bwd_out + jnp.einsum(
        "lhd,hde->lhe", bwd_reach, bwd_incoming, precision=lax.Precision.HIGHEST
    )
    attended = head_mix(fwd_full + bwd_full[::-1], head_norm_gain, output_gate_preact)
    token_rows = lax.all_to_all(attended, "tp", split_axis=0, concat_axis=1, tiled=True)
    whole_out = lax.all_gather(output_projection, "tp", axis=0, tiled=True)
    projected = jnp.dot(token_rows, whole_out, preferred_element_type=jnp.float32)
    mid_rows = (residual.astype(jnp.float32) + projected).astype(jnp.bfloat16)
    normed = row_norm(mid_rows, prenorm_gain)
    fetched = (
        lax.all_gather(gate_projection, "sp", axis=0, tiled=True),
        lax.all_gather(up_projection, "sp", axis=0, tiled=True),
        lax.all_gather(down_projection, "sp", axis=1, tiled=True),
    )
    gate_full, up_full, down_full = fetched
    piece = lax.all_gather(normed, "tp", axis=0, tiled=True)
    gate_part = jnp.dot(piece, gate_full, preferred_element_type=jnp.float32)
    up_part = jnp.dot(piece, up_full, preferred_element_type=jnp.float32)
    hidden = (jax.nn.silu(gate_part) * up_part).astype(jnp.bfloat16)
    summed = lax.psum_scatter(
        jnp.dot(hidden, down_full, preferred_element_type=jnp.float32).astype(jnp.bfloat16),
        "tp",
        scatter_dimension=0,
        tiled=True,
    ).astype(jnp.float32)
    return (mid_rows.astype(jnp.float32) + 0.5 * summed).astype(jnp.bfloat16)


def solution(mesh):
    in_specs = (
        P(("grp", "sp"), "tp"),
        P(("grp", "sp"), "tp"),
        P(("grp", "sp"), "tp"),
        P(("grp", "sp"), "tp"),
        P(("grp", "sp"), "tp"),
        P(("grp", "sp"), "tp"),
        P(None, "tp"),
        P("tp", ("grp", "sp")),
        P(("grp", "sp", "tp"), None),
        P("tp"),
        P("tp", None),
        P(),
        P("sp", "tp"),
        P("sp", "tp"),
        P("tp", "sp"),
    )
    out_specs = P(("grp", "sp", "tp"), None)
    return jax.shard_map(body, mesh=mesh, in_specs=in_specs, out_specs=out_specs, check_vma=False)
```

profile of v0, /device:TPU:0, one launch (start us, length us, event | category | flops | bytes accessed | tf_op | source)
XLA Modules:
  0.0 782.6 jit_solution(11281532606499490096)
XLA Ops:
  31.3 173.5 %while.62 = (s32[]{:T(128)}, f32[2,64,128]{2,1,0:T(8,128)S(1)}, f32[2,64]{1,0:T(2,128)S(1)}, f32[12,2,64,128]{3,2,0,1:T(8,128)S(1)}, f32[12,2,64,64]{3,2,1,0:T(8...) while((s32[]{:T(128)}, f32[2,64,128]{2,1,0:T(8,128)S(1)}, ...), condition=%wide.region_2.3_spmd.clone, body=%wide.region_0.2_spmd.clone.sunk | while | flops 41005312 | bytes 10040985 | solution.py:75
  34.4 5.6 copy.189
  45.8 3.0 select_exponential_fusion.4
  48.8 5.6 copy.189
  55.5 3.2 fusion.109
  60.6 3.0 select_exponential_fusion.4
  63.6 5.6 copy.189
  78.1 5.6 copy.189
  92.5 5.6 copy.189
  104.0 3.0 select_exponential_fusion.4
  107.0 5.6 copy.189
  121.4 5.6 copy.189
  132.9 3.0 select_exponential_fusion.4
  135.8 5.6 copy.189
  150.3 5.6 copy.189
  161.7 3.0 select_exponential_fusion.4
  164.7 5.6 copy.189
  179.1 5.6 copy.189
  193.5 5.6 copy.189
  205.8 209.2 %while.63 = (s32[]{:T(128)}, f32[2,64,128]{2,1,0:T(8,128)S(1)}, f32[2,64]{1,0:T(2,128)S(1)}, f32[12,2,64,128]{3,2,0,1:T(8,128)S(1)}, f32[12,2,64,64]{3,2,1,0:T(8...) while((s32[]{:T(128)}, f32[2,64,128]{2,1,0:T(8,128)S(1)}, ...), condition=%wide.region_7.8_spmd.clone, body=%wide.region_5.7_spmd.clone.sunk | while | flops 41005312 | bytes 9845901 | solution.py:75
  210.1 5.6 copy.195
  227.5 5.6 copy.195
  245.0 5.6 copy.195
  262.4 5.6 copy.195
  279.8 5.6 copy.195
  297.3 5.6 copy.195
  311.7 3.0 select_exponential_fusion.5
  314.7 5.6 copy.195
  332.1 5.6 copy.195
  349.6 5.6 copy.195
  364.0 3.0 select_exponential_fusion.5
  367.0 5.6 copy.195
  381.5 3.0 select_exponential_fusion.5
  384.4 5.6 copy.195
  401.9 5.6 copy.195
  419.2 12.9 %all-gather.5 = bf16[4,2,64]{2,1,0:T(2,128)(2,1)S(1)} all-gather(bf16[1,2,64]{2,1,0:T(2,128)(2,1)S(1)} %fusion.66), channel_id=4, replica_groups=mesh['grp'=2,'sp'=4,'tp'=4] {'sp'}, dimensions={0}, use_global_device_ids=true | all-gather | bytes 1280 | tf_op jit(solution)/shard_map/all_gather | solution.py:18
  432.1 13.4 %all-gather.3 = bf16[8,64,128]{2,1,0:T(8,128)(2,1)S(1)} all-gather(bf16[2,64,128]{2,1,0:T(8,128)(2,1)S(1)} %convert_element_type.105), channel_id=5, replica_groups=mesh['grp'=2,'sp'=4,'tp'=4] {'sp'}, dimensions={0}, use_global_device_ids=true | all-gather | bytes 163840 | tf_op jit(solution)/shard_map/all_gather | solution.py:18
  447.8 7.3 rev.19
  457.3 7.6 all-gather.4
  464.9 13.3 %all-gather.1 = bf16[8,64,128]{2,1,0:T(8,128)(2,1)S(1)} all-gather(bf16[2,64,128]{2,1,0:T(8,128)(2,1)S(1)} %convert_element_type.103), channel_id=3, replica_groups=mesh['grp'=2,'sp'=4,'tp'=4] {'sp'}, dimensions={0}, use_global_device_ids=true | all-gather | bytes 163840 | tf_op jit(solution)/shard_map/all_gather | solution.py:18
  481.3 10.0 %all_to_all.16 = bf16[4,192,256]{2,1,0:T(8,128)(2,1)S(1)} all-to-all(bf16[4,192,256]{2,1,0:T(8,128)(2,1)S(1)} %convert_element_type.107), channel_id=1, replica_groups=mesh['grp'=2,'sp'=4,'tp'=4] {'tp'}, dimensions={0} | all-to-all | bytes 786432 | tf_op jit(solution)/shard_map/all_to_all | solution.py:177
  491.3 3.5 multiply_reduce_fusion
  497.2 26.7 %all-gather.14.cloned.1.call-done = bf16[768,2048]{1,0:T(8,128)(2,1)} async-done(((bf16[192,2048]{1,0:T(8,128)(2,1)}), bf16[768,2048]{1,0:T(8,128)(2,1)}) %all-gather.14.cloned.1.call-update) | async-done | bytes 3145744 | tf_op jit(solution)/shard_map/all_gather | solution.py:188
  523.9 9.6 %fusion.70 = f32[768,1280]{1,0:T(8,128)} fusion(bf16[768,2048]{1,0:T(8,128)(2,1)} %all-gather.14.cloned.1.call-done, bf16[2048,1280]{1,0:T(8,128)(2,1)} %all-gather.16.cloned.1.call-done), kind=kOutput, calls=%fused_computation.119 | convolution fusion | flops 4026531840 | bytes 12320768 | tf_op jit(solution)/shard_map/dot_general | solution.py:189
  533.4 89.9 %all-gather.18.cloned.1.call-done = bf16[2048,1280]{1,0:T(8,128)(2,1)} async-done(((bf16[512,1280]{1,0:T(8,128)(2,1)}), bf16[2048,1280]{1,0:T(8,128)(2,1)}) %all-gather.18.cloned.1.call-update) | async-done | bytes 5242896 | tf_op jit(solution)/shard_map/all_gather | solution.py:184
  623.4 97.8 %all-gather.20.cloned.1.call-done = bf16[1280,2048]{1,0:T(8,128)(2,1)} async-done(((bf16[1280,512]{1,0:T(8,128)(2,1)}), bf16[1280,2048]{1,0:T(8,128)(2,1)}) %all-gather.20.cloned.1.call-update) | async-done | bytes 5242896 | tf_op jit(solution)/shard_map/all_gather | solution.py:185
  721.2 16.0 %convolution_convert_fusion = bf16[768,2048]{1,0:T(8,128)(2,1)} fusion(bf16[1280,2048]{1,0:T(8,128)(2,1)} %all-gather.20.cloned.1.call-done, bf16[768,2048]{1,0:T(8,128)(2,1)} %all-gather.14.cloned.1.call-done, bf16[2048,1280]{1,0:T(8,128)(2,1)} %all-gather.18.cloned.1.call-done, f32[768,1280]{1,0:T(8,128)} %fusion.70), kind=kOutput, calls=%fused_computation.75 | convolution fusion | flops 8060534784 | bytes 20709376 | tf_op jit(solution)/shard_map/dot_general | solution.py:193
  737.2 36.4 %reduce-scatter.2.cloned.1.call-done = bf16[192,2048]{1,0:T(8,128)(2,1)} async-done(((bf16[768,2048]{1,0:T(8,128)(2,1)}), bf16[192,2048]{1,0:T(8,128)(2,1)}) %reduce-scatter.2.cloned.1.call-update) | async-done | bytes 786448 | tf_op jit(solution)/shard_map/reduce_scatter | solution.py:192
  (465 shorter events, 261.1 us)
Async XLA Ops:
  6.5 3.0 copy-start.3
  6.5 4.8 copy-start.9
  6.5 4.9 copy-start.4
  6.5 5.0 copy-start.6
  6.5 484.8 %all-gather.12.cloned.1.call-start = ((), (), s32[]{:S(2)}) async-start(), calls=%async_computation.2 | async-start | bytes 5242880 | tf_op jit(solution)/shard_map/all_gather | solution.py:178
  7.3 489.9 %all-gather.16.cloned.1.call-start = ((), (), s32[]{:S(2)}) async-start(), calls=%async_computation.4 | async-start | bytes 6553600 | tf_op jit(solution)/shard_map/all_gather | solution.py:183
  8.0 515.9 %all-gather.14.cloned.1.call-start = ((), (), s32[]{:S(2)}) async-start(), calls=%async_computation.3 | async-start | bytes 3932160 | tf_op jit(solution)/shard_map/all_gather | solution.py:188
  11.8 8.5 %copy-start.5 = (bf16[768,128]{1,0:T(8,128)(2,1)S(1)}, bf16[768,128]{1,0:T(8,128)(2,1)}, u32[]{:S(2)}) copy-start(bf16[768,128]{1,0:T(8,128)(2,1)} %param.23) | copy-start | bytes 589828
  415.0 0.9 copy-start
  447.8 9.3 %copy-start.2 = (bf16[768,256]{1,0:T(8,128)(2,1)S(1)}, bf16[768,256]{1,0:T(8,128)(2,1)}, u32[]{:S(2)}) copy-start(bf16[768,256]{1,0:T(8,128)(2,1)} %param.26) | copy-start | bytes 1179652
  455.6 22.6 %copy-start.1 = (f32[768,2,128]{0,2,1:T(8,128)S(1)}, f32[768,2,128]{0,2,1:T(8,128)}, u32[]{:S(2)}) copy-start(f32[768,2,128]{0,2,1:T(8,128)} %rev.19) | copy-start | bytes 2359300
  455.7 24.6 %copy-start.8 = (f32[256]{0:T(256)S(1)}, f32[256]{0:T(256)}, u32[]{:S(2)}) copy-start(f32[256]{0:T(256)} %param.32) | copy-start | bytes 3076
  481.3 13.6 %copy-start.7 = (f32[2048]{0:T(1024)S(1)}, f32[2048]{0:T(1024)}, u32[]{:S(2)}) copy-start(f32[2048]{0:T(1024)} %param.34) | copy-start | bytes 24580
  496.0 127.4 %all-gather.18.cloned.1.call-start = ((), (), s32[]{:S(2)}) async-start(), calls=%async_computation.5 | async-start | bytes 6553600 | tf_op jit(solution)/shard_map/all_gather | solution.py:184
  496.6 224.6 %all-gather.20.cloned.1.call-start = ((), (), s32[]{:S(2)}) async-start(), calls=%async_computation.6 | async-start | bytes 6553600 | tf_op jit(solution)/shard_map/all_gather | solution.py:185
  497.1 276.4 %reduce-scatter.2.cloned.1.call-start = ((), (), s32[]{:S(2)}) async-start(), calls=%async_computation.7 | async-start | bytes 3932160 | tf_op jit(solution)/shard_map/reduce_scatter | solution.py:192
Sparse Core Ops, SparseCore 0:
  8.9 37.1 all-gather.11
  47.7 98.0 all-gather.15
  496.1 27.7 all-gather.13
  525.3 98.0 all-gather.17
  624.8 96.3 all-gather.19
  737.3 36.1 reduce-scatter.1
where the time goes:
time: 788 us; the launch traced here: 783 us
  waiting for transfers between devices  253 us (32%)
  local copies, waits for them, and re-layouts  224 us (28%)
  other arithmetic  159 us (20%)
  matrix products  72.5 us (9%)
  blocking collectives  57.2 us (7%)
  between operations  13.9 us (2%)
    while x24, local copies, waits for them, and re-layouts  134 us
    all_gather x1, waiting for transfers between devices, body(): lax.all_gather(down_projection, 'sp', axis=1, tiled=True)  97.8 us
    all_gather x1, waiting for transfers between devices, body(): lax.all_gather(up_projection, 'sp', axis=0, tiled=True)  89.9 us
    exp x24, other arithmetic, advance(): jnp.exp(jnp.where(lower_mask, within[:, :, None, :] - within[:, None, :,...  71.7 us
    dot_general x24, other arithmetic, advance(): jnp.einsum('hid,hjd,hijd->hij', query_blk, key_blk, spread, precision=lax...  69 us
    dynamic_slice x108, local copies, waits for them, and re-layouts, block_sweep(): lax.scan(advance, (start_memory, start_offset), (blocks(key_in), blocks(v...  52.5 us
    all_gather x4, blocking collectives, entering(): lax.all_gather(a.astype(kind), axis)  47.2 us
    reduce_scatter x1, waiting for transfers between devices, body(): lax.psum_scatter(jnp.dot(hidden, down_full, preferred_element_type=jnp.fl...  36.4 us
  transfers between devices with their start and end apart: 6, of which 4 were waited for; matrix products, arithmetic and copies ran while one was open for 56% of the time, Pallas kernels for 0%

commit v1 on v0

--- a/solution.py
+++ b/solution.py
@@ -182,7 +182,7 @@
     fetched = (
         lax.all_gather(gate_projection, "sp", axis=0, tiled=True),
         lax.all_gather(up_projection, "sp", axis=0, tiled=True),
-        lax.all_gather(down_projection, "sp", axis=1, tiled=True),
+        jnp.concatenate(lax.all_gather(down_projection, "sp"), axis=1),
     )
     gate_full, up_full, down_full = fetched
     piece = lax.all_gather(normed, "tp", axis=0, tiled=True)

time: 788 us -> 691 us (0.88)
  waiting for transfers between devices: 253 us -> 148 us
  local copies, waits for them, and re-layouts: 224 us -> 232 us
    all_gather x1, waiting for transfers between devices: 97.8 us -> 0.02 us  [body(): lax.all_gather(down_projection, 'sp')]
    reshape x0 -> x1, local copies, waits for them, and re-layouts: none -> 7.98 us  [body(): jnp.concatenate(lax.all_gather(down_projection, 'sp'), axis=1)]
  transfers between devices with their start and end apart: 6 -> 6, of which waited for: 4 -> 3; matrix products, arithmetic and copies ran while one was open for 56% -> 65% of each run, Pallas kernels for 0% -> 0%
where the time goes in v1:
time: 691 us; the launch traced here: 686 us
  local copies, waits for them, and re-layouts  232 us (34%)
  other arithmetic  159 us (23%)
  waiting for transfers between devices  148 us (21%)
  matrix products  72.5 us (10%)
  blocking collectives  57 us (8%)
  between operations  13.8 us (2%)
    while x24, local copies, waits for them, and re-layouts  135 us
    all_gather x1, waiting for transfers between devices, body(): lax.all_gather(up_projection, 'sp', axis=0, tiled=True)  89.9 us
    exp x24, other arithmetic, advance(): jnp.exp(jnp.where(lower_mask, within[:, :, None, :] - within[:, None, :,...  71.7 us
    dot_general x24, other arithmetic, advance(): jnp.einsum('hid,hjd,hijd->hij', query_blk, key_blk, spread, precision=lax...  69 us
    dynamic_slice x108, local copies, waits for them, and re-layouts, block_sweep(): lax.scan(advance, (start_memory, start_offset), (blocks(key_in), blocks(v...  52.5 us
    all_gather x4, blocking collectives, entering(): lax.all_gather(a.astype(kind), axis)  47.1 us
    reduce_scatter x1, waiting for transfers between devices, body(): lax.psum_scatter(jnp.dot(hidden, down_full, preferred_element_type=jnp.fl...  36.4 us
    all_gather x1, waiting for transfers between devices, body(): piece = lax.all_gather(normed, 'tp', axis=0, tiled=True)  19.2 us
  transfers between devices with their start and end apart: 6, of which 3 were waited for; matrix products, arithmetic and copies ran while one was open for 65% of the time, Pallas kernels for 0%

profile of v1, /device:TPU:0, one launch (start us, length us, event | category | flops | bytes accessed | tf_op | source)
XLA Modules:
  0.0 685.6 jit_solution(13901278364404752746)
XLA Ops:
  32.0 173.7 %while.62 = (s32[]{:T(128)}, f32[2,64,128]{2,1,0:T(8,128)S(1)}, f32[2,64]{1,0:T(2,128)S(1)}, f32[12,2,64,128]{3,2,0,1:T(8,128)S(1)}, f32[12,2,64,64]{3,2,1,0:T(8...) while((s32[]{:T(128)}, f32[2,64,128]{2,1,0:T(8,128)S(1)}, ...), condition=%wide.region_2.3_spmd.clone, body=%wide.region_0.2_spmd.clone.sunk | while | flops 41005312 | bytes 10040985 | solution.py:75
  32.2 3.0 select_exponential_fusion.4
  35.2 5.6 copy.191
  46.6 3.0 select_exponential_fusion.4
  49.6 5.6 copy.191
  56.3 3.2 fusion.109
  61.4 3.0 select_exponential_fusion.4
  64.4 5.6 copy.191
  75.8 3.0 select_exponential_fusion.4
  78.8 5.6 copy.191
  90.3 3.0 select_exponential_fusion.4
  93.3 5.6 copy.191
  104.7 3.0 select_exponential_fusion.4
  107.7 5.6 copy.191
  119.1 3.0 select_exponential_fusion.4
  122.1 5.6 copy.191
  133.5 3.0 select_exponential_fusion.4
  136.5 5.6 copy.191
  150.9 5.8 copy.191
  165.6 5.6 copy.191
  180.0 5.6 copy.191
  194.5 5.6 copy.191
  206.8 209.1 %while.63 = (s32[]{:T(128)}, f32[2,64,128]{2,1,0:T(8,128)S(1)}, f32[2,64]{1,0:T(2,128)S(1)}, f32[12,2,64,128]{3,2,0,1:T(8,128)S(1)}, f32[12,2,64,64]{3,2,1,0:T(8...) while((s32[]{:T(128)}, f32[2,64,128]{2,1,0:T(8,128)S(1)}, ...), condition=%wide.region_7.8_spmd.clone, body=%wide.region_5.7_spmd.clone.sunk | while | flops 41005312 | bytes 9845901 | solution.py:75
  211.1 5.6 copy.197
  228.6 5.6 copy.197
  246.0 5.6 copy.197
  263.4 5.6 copy.197
  280.8 5.6 copy.197
  298.3 5.6 copy.197
  315.7 5.6 copy.197
  333.1 5.6 copy.197
  350.6 5.6 copy.197
  368.0 5.6 copy.197
  385.4 5.6 copy.197
  402.8 5.6 copy.197
  420.2 12.8 %all-gather.6 = bf16[4,2,64]{2,1,0:T(2,128)(2,1)S(1)} all-gather(bf16[1,2,64]{2,1,0:T(2,128)(2,1)S(1)} %fusion.66), channel_id=4, replica_groups=mesh['grp'=2,'sp'=4,'tp'=4] {'sp'}, dimensions={0}, use_global_device_ids=true | all-gather | bytes 1280 | tf_op jit(solution)/shard_map/all_gather | solution.py:18
  433.0 13.4 %all-gather.3 = bf16[8,64,128]{2,1,0:T(8,128)(2,1)S(1)} all-gather(bf16[2,64,128]{2,1,0:T(8,128)(2,1)S(1)} %convert_element_type.105), channel_id=5, replica_groups=mesh['grp'=2,'sp'=4,'tp'=4] {'sp'}, dimensions={0}, use_global_device_ids=true | all-gather | bytes 163840 | tf_op jit(solution)/shard_map/all_gather | solution.py:18
  448.7 7.3 %rev.19 = f32[768,2,128]{0,2,1:T(8,128)} reverse(f32[768,2,128]{0,2,1:T(8,128)} %fusion.48), dimensions={0} | reverse | bytes 1572864 | tf_op jit(solution)/shard_map/rev | solution.py:176
  458.2 7.6 %all-gather.5 = bf16[4,2,64]{2,1,0:T(2,128)(2,1)S(1)} all-gather(bf16[1,2,64]{2,1,0:T(2,128)(2,1)S(1)} %fusion.65), channel_id=2, replica_groups=mesh['grp'=2,'sp'=4,'tp'=4] {'sp'}, dimensions={0}, use_global_device_ids=true | all-gather | bytes 1280 | tf_op jit(solution)/shard_map/all_gather | solution.py:18
  465.8 13.3 %all-gather.1 = bf16[8,64,128]{2,1,0:T(8,128)(2,1)S(1)} all-gather(bf16[2,64,128]{2,1,0:T(8,128)(2,1)S(1)} %convert_element_type.103), channel_id=3, replica_groups=mesh['grp'=2,'sp'=4,'tp'=4] {'sp'}, dimensions={0}, use_global_device_ids=true | all-gather | bytes 163840 | tf_op jit(solution)/shard_map/all_gather | solution.py:18
  482.2 9.9 %all_to_all.16 = bf16[4,192,256]{2,1,0:T(8,128)(2,1)S(1)} all-to-all(bf16[4,192,256]{2,1,0:T(8,128)(2,1)S(1)} %convert_element_type.107), channel_id=1, replica_groups=mesh['grp'=2,'sp'=4,'tp'=4] {'tp'}, dimensions={0} | all-to-all | bytes 786432 | tf_op jit(solution)/shard_map/all_to_all | solution.py:177
  492.2 3.5 multiply_reduce_fusion
  497.5 8.0 %copy.121 = bf16[1280,4,512]{0,2,1:T(8,128)(2,1)} copy(bf16[1280,4,512]{2,0,1:T(8,128)(2,1)} %bitcast.244) | data formatting | bytes 10485760 | tf_op jit(solution)/shard_map/reshape | solution.py:185
  505.5 19.2 %all-gather.15.cloned.1.call-done = bf16[768,2048]{1,0:T(8,128)(2,1)} async-done(((bf16[192,2048]{1,0:T(8,128)(2,1)}), bf16[768,2048]{1,0:T(8,128)(2,1)}) %all-gather.15.cloned.1.call-update) | async-done | bytes 3145744 | tf_op jit(solution)/shard_map/all_gather | solution.py:188
  524.7 9.6 %fusion.70 = f32[768,1280]{1,0:T(8,128)} fusion(bf16[768,2048]{1,0:T(8,128)(2,1)} %all-gather.15.cloned.1.call-done, bf16[2048,1280]{1,0:T(8,128)(2,1)} %all-gather.17.cloned.1.call-done), kind=kOutput, calls=%fused_computation.119 | convolution fusion | flops 4026531840 | bytes 12320768 | tf_op jit(solution)/shard_map/dot_general | solution.py:189
  534.3 89.9 %all-gather.19.cloned.1.call-done = bf16[2048,1280]{1,0:T(8,128)(2,1)} async-done(((bf16[512,1280]{1,0:T(8,128)(2,1)}), bf16[2048,1280]{1,0:T(8,128)(2,1)}) %all-gather.19.cloned.1.call-update) | async-done | bytes 5242896 | tf_op jit(solution)/shard_map/all_gather | solution.py:184
  624.2 16.0 %convolution_convert_fusion = bf16[768,2048]{1,0:T(8,128)(2,1)} fusion(bf16[1280,2048]{0,1:T(8,128)(2,1)} %bitcast.245, bf16[768,2048]{1,0:T(8,128)(2,1)} %all-gather.15.cloned.1.call-done, bf16[2048,1280]{1,0:T(8,128)(2,1)} %all-gather.19.cloned.1.call-done, f32[768,1280]{1,0:T(8,128)} %fusion.70), kind=kOutput, calls=%fused_computation.75 | convolution fusion | flops 8060534784 | bytes 20709376 | tf_op jit(solution)/shard_map/dot_general | solution.py:193
  640.2 36.4 %reduce-scatter.2.cloned.1.call-done = bf16[192,2048]{1,0:T(8,128)(2,1)} async-done(((bf16[768,2048]{1,0:T(8,128)(2,1)}), bf16[192,2048]{1,0:T(8,128)(2,1)}) %reduce-scatter.2.cloned.1.call-update) | async-done | bytes 786448 | tf_op jit(solution)/shard_map/reduce_scatter | solution.py:192
  (466 shorter events, 261.4 us)
Async XLA Ops:
  6.5 3.7 copy-start.3
  6.5 485.7 %all-gather.13.cloned.1.call-start = ((), (), s32[]{:S(2)}) async-start(), calls=%async_computation.2 | async-start | bytes 5242880 | tf_op jit(solution)/shard_map/all_gather | solution.py:178
  6.5 5.5 copy-start.9
  6.5 5.6 copy-start.4
  6.5 5.8 copy-start.6
  7.3 490.3 %all-gather.21.cloned.1.call-start = ((), (), s32[]{:S(2)}) async-start(), calls=%async_computation.7 | async-start | bytes 6553600 | tf_op jit(solution)/shard_map/all_gather | solution.py:185
  8.0 497.5 %all-gather.17.cloned.1.call-start = ((), (), s32[]{:S(2)}) async-start(), calls=%async_computation.4 | async-start | bytes 6553600 | tf_op jit(solution)/shard_map/all_gather | solution.py:183
  8.7 515.9 %all-gather.15.cloned.1.call-start = ((), (), s32[]{:S(2)}) async-start(), calls=%async_computation.3 | async-start | bytes 3932160 | tf_op jit(solution)/shard_map/all_gather | solution.py:188
  12.5 8.5 %copy-start.5 = (bf16[768,128]{1,0:T(8,128)(2,1)S(1)}, bf16[768,128]{1,0:T(8,128)(2,1)}, u32[]{:S(2)}) copy-start(bf16[768,128]{1,0:T(8,128)(2,1)} %param.23) | copy-start | bytes 589828
  416.0 0.9 copy-start
  448.7 9.3 %copy-start.2 = (bf16[768,256]{1,0:T(8,128)(2,1)S(1)}, bf16[768,256]{1,0:T(8,128)(2,1)}, u32[]{:S(2)}) copy-start(bf16[768,256]{1,0:T(8,128)(2,1)} %param.26) | copy-start | bytes 1179652
  456.5 22.6 %copy-start.1 = (f32[768,2,128]{0,2,1:T(8,128)S(1)}, f32[768,2,128]{0,2,1:T(8,128)}, u32[]{:S(2)}) copy-start(f32[768,2,128]{0,2,1:T(8,128)} %rev.19) | copy-start | bytes 2359300
  456.5 24.6 %copy-start.8 = (f32[256]{0:T(256)S(1)}, f32[256]{0:T(256)}, u32[]{:S(2)}) copy-start(f32[256]{0:T(256)} %param.32) | copy-start | bytes 3076
  482.2 13.6 %copy-start.7 = (f32[2048]{0:T(1024)S(1)}, f32[2048]{0:T(1024)}, u32[]{:S(2)}) copy-start(f32[2048]{0:T(1024)} %param.34) | copy-start | bytes 24580
  496.9 127.3 %all-gather.19.cloned.1.call-start = ((), (), s32[]{:S(2)}) async-start(), calls=%async_computation.5 | async-start | bytes 6553600 | tf_op jit(solution)/shard_map/all_gather | solution.py:184
  497.5 179.1 %reduce-scatter.2.cloned.1.call-start = ((), (), s32[]{:S(2)}) async-start(), calls=%async_computation.6 | async-start | bytes 3932160 | tf_op jit(solution)/shard_map/reduce_scatter | solution.py:192
Sparse Core Ops, SparseCore 0:
  8.9 37.2 all-gather.12
  47.7 97.9 all-gather.20
  147.3 96.3 all-gather.16
  497.0 27.6 all-gather.14
  526.1 98.0 all-gather.18
  640.3 36.1 reduce-scatter.1
